TPU v7x, 32 devices: a whole 2x2x4 slice. The times are simulated.
32 devices in a mesh: sp: 8 (over z, y), tp: 4 (over x, core).
Axes of the slice: x: 2, y: 2, z: 4, core: 2. Of those that a mesh axis runs over, the one named last changes fastest.
Arguments:
- queries_nope: bfloat16 [3072, 8, 128], P('sp', 'tp'), may hold values from -9 to 9
- queries_rope: bfloat16 [3072, 8, 64], P('sp', 'tp'), may hold values from -6 to 6
- latent: bfloat16 [3072, 512], P('sp'), may hold values from -8 to 8, as said below
- rope_key: bfloat16 [3072, 64], P('sp'), may hold values from -6 to 6
- latent_gain: float32 [512], replicated, may hold values from 0.1 to 1.9
- key_up: bfloat16 [512, 1024], P(None, 'tp'), may hold values from -0.25 to 0.25
- value_up: bfloat16 [512, 1024], P(None, 'tp'), may hold values from -0.25 to 0.25
- out_proj: bfloat16 [1024, 2048], P('tp'), may hold values from -0.75 to 0.75
- stream: bfloat16 [3072, 2048], P(('sp', 'tp')), may hold values from -6 to 6
- mix_gain: float32 [2048], replicated, may hold values from 0.1 to 1.9
- w_gate: bfloat16 [2048, 3072], P('sp', 'tp'), may hold values from -0.125 to 0.125
- w_up: bfloat16 [2048, 3072], P('sp', 'tp'), may hold values from -0.125 to 0.125
- w_down: bfloat16 [3072, 2048], P('tp', 'sp'), may hold values from -0.4375 to 0.4375
- mlp_gain: float32 [2048], replicated, may hold values from 0.1 to 1.9
Outputs:
- result: bfloat16 [3072, 2048], P(('sp', 'tp'))
Inputs may be any that keep to these rules, and one draw needn't show every extreme that they name: latent rows carry a mean vector that changes from one eighth of the sequence to the next.
All inputs are finite; a program needn't handle non-finite values.
Results may differ from a plain program's by a relative error of at most 0.017.
Values may be sent and summed in bfloat16 or wider, within the bound.
A program may use at most 192 MiB of HBM per device.

v0:
```python
import jax
import jax.numpy as jnp
from jax import lax
from jax.sharding import PartitionSpec as P

theta_base = 10000.0
residual_weight = 8.0**0.25
norm_floor = 1.0
big_negative = -1e30


def rotate(vector, first_row):
    half = vector.shape[-1] // 2
    rates = theta_base ** (-2.0 * jnp.arange(half, dtype=jnp.float32) / vector.shape[-1])
    places = (first_row + jnp.arange(vector.shape[0], dtype=jnp.int32)).astype(jnp.float32)
    angle = places[:, None] * rates[None, :]
    angle = angle.reshape((vector.shape[0],) + (1,) * (vector.ndim - 2) + (half,))
    cosine = jnp.cos(angle)
    sine = jnp.sin(angle)
    left = vector[..., :half]
    right = vector[..., half:]
    return jnp.concatenate([left * cosine - right * sine, left * sine + right * cosine], axis=-1)


def latent_norm(latent, latent_gain):
    wide = latent.astype(jnp.float32)
    factor = lax.rsqrt(jnp.mean(wide * wide, axis=-1, keepdims=True) + norm_floor)
    return (wide * factor * latent_gain).astype(jnp.bfloat16)


def layer_norm(values, gain):
    centre = jnp.mean(values, axis=-1, keepdims=True)
    centred = values - centre
    spread = jnp.mean(centred * centred, axis=-1, keepdims=True)
    return centred * lax.rsqrt(spread + norm_floor) * gain


def per_device(
    queries_nope,
    queries_rope,
    latent,
    rope_key,
    latent_gain,
    key_up,
    value_up,
    out_proj,
    stream,
    mix_gain,
    w_gate,
    w_up,
    w_down,
    mlp_gain,
):
    row_count, head_count, head_dim = queries_nope.shape
    rope_dim = queries_rope.shape[2]
    first_row = lax.axis_index("sp") * row_count
    query_turned = rotate(queries_rope.astype(jnp.float32), first_row).astype(jnp.bfloat16)
    key_turned = rotate(rope_key.astype(jnp.float32), first_row).astype(jnp.bfloat16)
    normed = latent_norm(latent, latent_gain)
    scale = (head_dim + rope_dim) ** (-0.5)
    query_places = first_row + jnp.arange(row_count, dtype=jnp.int32)
    last_place = first_row + row_count - 1

    def add_piece(carry, piece):
        top, denominators, weighted = carry
        latent_piece, rotary_piece = piece
        count = latent_piece.shape[0]
        keys = jnp.dot(latent_piece, key_up, preferred_element_type=jnp.float32).astype(
            jnp.bfloat16
        )
        keys = keys.reshape(count, head_count, head_dim)
        values_here = jnp.dot(latent_piece, value_up, preferred_element_type=jnp.float32).astype(
            jnp.bfloat16
        )
        values_here = values_here.reshape(count, head_count, head_dim)
        score = jnp.einsum("thd,shd->hts", queries_nope, keys, preferred_element_type=jnp.float32)
        score = score + jnp.einsum(
            "thr,sr->hts", query_turned, rotary_piece, preferred_element_type=jnp.float32
        )
        score = score * scale
        allowed = jnp.arange(count, dtype=jnp.int32)[None, :] <= query_places[:, None]
        score = jnp.where(allowed[None], score, big_negative)
        new_top = jnp.maximum(top, jnp.max(score, axis=2))
        powers = jnp.exp(score - new_top[:, :, None]) * allowed[None]
        shrink = jnp.exp(top - new_top)
        denominators = jnp.sum(powers, axis=2)
        weighted = weighted * shrink.T[:, :, None] + jnp.einsum(
            "hts,shd->thd",
            powers.astype(jnp.bfloat16),
            values_here,
            preferred_element_type=jnp.float32,
        )
        return (new_top, denominators, weighted)

    start_state = (
        jnp.full((head_count, row_count), big_negative, jnp.float32),
        jnp.zeros((head_count, row_count), jnp.float32),
        jnp.zeros((row_count, head_count, head_dim), jnp.float32),
    )
    piece = (
        lax.all_gather(normed, "sp", axis=0, tiled=True),
        lax.all_gather(key_turned, "sp", axis=0, tiled=True),
    )
    top, denominators, weighted = lax.cond(
        jnp.int32(0) <= last_place,
        lambda state: add_piece(state, piece),
        lambda state: state,
        start_state,
    )
    attended = (
        (weighted / denominators.T[:, :, None])
        .astype(jnp.bfloat16)
        .reshape(row_count, head_count * head_dim)
    )
    row_heads = lax.all_to_all(attended, "tp", split_axis=0, concat_axis=1, tiled=True)
    whole_proj = lax.all_gather(out_proj, "tp", axis=0, tiled=True)
    projected = jnp.dot(row_heads, whole_proj, preferred_element_type=jnp.float32)
    mixed = layer_norm(residual_weight * stream.astype(jnp.float32) + projected, mix_gain).astype(
        jnp.bfloat16
    )
    all_rows = lax.all_gather(mixed, "tp", axis=0, tiled=True)
    gate_sum = jnp.dot(
        all_rows,
        lax.all_gather(w_gate, "sp", axis=0, tiled=True),
        preferred_element_type=jnp.float32,
    )
    up_sum = jnp.dot(
        all_rows, lax.all_gather(w_up, "sp", axis=0, tiled=True), preferred_element_type=jnp.float32
    )
    hidden = (jax.nn.silu(gate_sum) * up_sum).astype(jnp.bfloat16)
    terms = jnp.dot(
        hidden, lax.all_gather(w_down, "sp", axis=1, tiled=True), preferred_element_type=jnp.float32
    )
    lowered = lax.psum_scatter(
        terms.astype(jnp.bfloat16), "tp", scatter_dimension=0, tiled=True
    ).astype(jnp.float32)
    return layer_norm(residual_weight * mixed.astype(jnp.float32) + 0.5 * lowered, mlp_gain).astype(
        jnp.bfloat16
    )


def solution(mesh):
    return jax.shard_map(
        per_device,
        mesh=mesh,
        in_specs=(
            P("sp", "tp", None),
            P("sp", "tp", None),
            P("sp", None),
            P("sp", None),
            P(),
            P(None, "tp"),
            P(None, "tp"),
            P("tp", None),
            P(("sp", "tp"), None),
            P(),
            P("sp", "tp"),
            P("sp", "tp"),
            P("tp", "sp"),
            P(),
        ),
        out_specs=P(("sp", "tp"), None),
        check_vma=False,
    )
```

profile of v0, /device:TPU:27, one launch (start us, length us, event | category | flops | bytes accessed | tf_op | source)
XLA Modules:
  0.0 362.7 jit_solution(3936866935383197673)
XLA Ops:
  6.5 0.0 copy-start.6
  6.5 0.0 copy-start.4
  6.5 0.0 copy-start.2
  6.5 0.0 all-gather.7.cloned.1.call-start
  6.5 1.2 fusion.19
  7.8 1.9 fusion.21
  9.7 0.0 all-gather.7.cloned.1.call-update
  9.7 0.0 all-gather.9.cloned.1.call-start
  9.7 0.7 all-gather.9.cloned.1.call-update
  10.5 0.0 all-gather.13.cloned.1.call-start
  10.5 0.7 all-gather.13.cloned.1.call-update
  11.2 0.0 all-gather.11.cloned.1.call-start
  11.2 0.8 convert_element_type.70
  12.0 0.0 copy-done.6
  12.1 0.3 multiply_cosine_fusion
  12.5 25.2 %all_gather.22 = bf16[3072,64]{0,1:T(8,128)(2,1)} all-gather(bf16[384,64]{0,1:T(8,128)(2,1)S(1)} %pad_maximum_fusion.1), channel_id=1, replica_groups=mesh['sp'=8,'tp'=4] {'sp'}, dimensions={0}, use_global_device_ids=true | all-gather | bytes 442368 | tf_op jit(solution)/shard_map/all_gather | solution.py:102
  37.7 34.0 %all-gather.7.cloned.1.call-done = bf16[3072,512]{1,0:T(8,128)(2,1)} async-done(((bf16[384,512]{1,0:T(8,128)(2,1)}), bf16[3072,512]{1,0:T(8,128)(2,1)}) %all-gather.7.cloned.1.call-update) | async-done | bytes 3145744 | tf_op jit(solution)/shard_map/all_gather | solution.py:101
  71.7 0.0 copy-done.4
  71.7 0.0 copy-done.2
  71.7 12.4 %conditional.1 = (f32[2,384]{1,0:T(2,128)S(1)}, f32[384,2,128]{0,2,1:T(8,128)S(1)}) conditional(s32[]{:T(128)} %convert_element_type.67, () %tuple.13, (s32[]{:T(128)}, s32[384]{0:T(512)S(1)}, bf16[3072,512]{1,0:T(8,128)(2,1)}, bf16[512,256]{1,0:T(8,128)(2,1)S(1)}, bf16[384,2,128]{2,1,0:T(2,128)(2,1)S(1)}, /*index=5*/bf16[3072,64]{0,1:T(8,128)(2,1)}, ...), branch_computations={%region_1.0_spmd, %region_2.5_spmd} | conditional | flops 3148186624 | bytes 93123176 | solution.py:104
  71.7 2.9 convolution_convert_fusion.1
  74.6 1.6 fusion.15
  76.1 0.0 copy-start.1
  76.2 1.0 fusion.17
  77.1 0.0 copy-done.1
  77.2 0.0 copy-start
  77.2 0.0 copy-start.3
  77.2 2.4 fusion.25
  79.6 0.0 copy-done
  79.6 0.0 copy-done.3
  79.6 1.1 convolution_convert_fusion
  80.7 1.9 fusion.11
  82.5 1.5 fusion.3
  84.1 0.2 copy.24
  84.3 0.1 all_to_all.14
  84.4 10.1 %all_to_all.19 = bf16[4,96,256]{2,1,0:T(8,128)(2,1)S(1)} all-to-all(bf16[4,96,256]{2,1,0:T(8,128)(2,1)S(1)} %all_to_all.14), channel_id=1, replica_groups=mesh['sp'=8,'tp'=4] {'tp'}, dimensions={0} | all-to-all | bytes 393216 | tf_op jit(solution)/shard_map/all_to_all | solution.py:115
  94.6 15.7 %all-gather.9.cloned.1.call-done = bf16[1024,2048]{1,0:T(8,128)(2,1)} async-done(((bf16[256,2048]{1,0:T(8,128)(2,1)}), bf16[1024,2048]{1,0:T(8,128)(2,1)}) %all-gather.9.cloned.1.call-update) | async-done | bytes 4194320 | tf_op jit(solution)/shard_map/all_gather | solution.py:116
  110.2 0.0 copy-start.5
  110.2 3.2 fusion.26
  113.4 0.2 multiply_reduce_fusion.1
  113.7 0.0 copy-done.5
  113.7 0.9 multiply_convert_fusion.1
  114.6 0.0 all-gather.11.cloned.1.call-update
  114.6 0.0 all-gather.15.cloned.1.call-start
  114.7 0.5 all-gather.15.cloned.1.call-update
  115.2 0.0 all-gather.17.cloned.1.call-start
  115.3 0.5 all-gather.17.cloned.1.call-update
  115.8 0.0 reduce-scatter.2.cloned.1.call-start
  115.9 55.5 %all-gather.13.cloned.1.call-done = bf16[2048,768]{1,0:T(8,128)(2,1)} async-done(((bf16[256,768]{1,0:T(8,128)(2,1)}), bf16[2048,768]{1,0:T(8,128)(2,1)}) %all-gather.13.cloned.1.call-update) | async-done | bytes 3145744 | tf_op jit(solution)/shard_map/all_gather | solution.py:124
  171.4 20.8 %all-gather.11.cloned.1.call-done = bf16[384,2048]{1,0:T(8,128)(2,1)} async-done(((bf16[96,2048]{1,0:T(8,128)(2,1)}), bf16[384,2048]{1,0:T(8,128)(2,1)}) %all-gather.11.cloned.1.call-update) | async-done | bytes 1572880 | tf_op jit(solution)/shard_map/all_gather | solution.py:121
  192.2 0.0 copy-start.8
  192.2 4.9 %fusion.27 = f32[384,768]{1,0:T(8,128)} fusion(bf16[384,2048]{1,0:T(8,128)(2,1)} %all-gather.11.cloned.1.call-done, bf16[2048,768]{1,0:T(8,128)(2,1)} %all-gather.13.cloned.1.call-done), kind=kOutput, calls=%fused_computation.56 | convolution fusion | flops 1207959552 | bytes 5898240 | tf_op jit(solution)/shard_map/dot_general | solution.py:122
  197.1 56.1 %all-gather.15.cloned.1.call-done = bf16[2048,768]{1,0:T(8,128)(2,1)} async-done(((bf16[256,768]{1,0:T(8,128)(2,1)}), bf16[2048,768]{1,0:T(8,128)(2,1)}) %all-gather.15.cloned.1.call-update) | async-done | bytes 3145744 | tf_op jit(solution)/shard_map/all_gather | solution.py:128
  253.2 63.0 %all-gather.17.cloned.1.call-done = bf16[768,2048]{1,0:T(8,128)(2,1)} async-done(((bf16[768,256]{1,0:T(8,128)(2,1)}), bf16[768,2048]{1,0:T(8,128)(2,1)}) %all-gather.17.cloned.1.call-update) | async-done | bytes 3145744 | tf_op jit(solution)/shard_map/all_gather | solution.py:132
  316.2 0.0 copy-done.8
  316.2 7.5 %convolution_convert_fusion.2 = bf16[384,2048]{1,0:T(8,128)(2,1)} fusion(bf16[768,2048]{1,0:T(8,128)(2,1)} %all-gather.17.cloned.1.call-done, bf16[384,2048]{1,0:T(8,128)(2,1)S(1)} %copy-done.8, bf16[2048,768]{1,0:T(8,128)(2,1)} %all-gather.15.cloned.1.call-done, f32[384,768]{1,0:T(8,128)} %fusion.27), kind=kOutput, calls=%fused_computation.21 | convolution fusion | flops 2418475008 | bytes 10616832 | tf_op jit(solution)/shard_map/dot_general | solution.py:131
  323.7 0.0 copy-start.7
  323.7 0.0 reduce-scatter.2.cloned.1.call-update
  323.7 27.1 %reduce-scatter.2.cloned.1.call-done = bf16[96,2048]{1,0:T(8,128)(2,1)} async-done(((bf16[384,2048]{1,0:T(8,128)(2,1)}), bf16[96,2048]{1,0:T(8,128)(2,1)}) %reduce-scatter.2.cloned.1.call-update) | async-done | bytes 393232 | tf_op jit(solution)/shard_map/reduce_scatter | solution.py:134
  350.8 1.4 fusion.23
  352.2 1.4 multiply_reduce_fusion
  353.6 0.0 copy-done.7
  353.6 2.2 multiply_convert_fusion
  (16 shorter events, 0.2 us)
Async XLA Ops:
  6.5 5.5 %copy-start.6 = (bf16[384,2,64]{0,2,1:T(8,128)(2,1)S(1)}, bf16[384,2,64]{0,2,1:T(8,128)(2,1)}, u32[]{:S(2)}) copy-start(bf16[384,2,64]{0,2,1:T(8,128)(2,1)} %param.17) | copy-start | bytes 294916
  6.5 65.1 %copy-start.4 = (bf16[384,2,128]{2,1,0:T(2,128)(2,1)S(1)}, bf16[384,2,128]{2,1,0:T(2,128)(2,1)}, u32[]{:S(2)}) copy-start(bf16[384,2,128]{2,1,0:T(2,128)(2,1)} %param.16) | copy-start | bytes 589828
  6.5 65.1 %copy-start.2 = (bf16[512,256]{1,0:T(8,128)(2,1)S(1)}, bf16[512,256]{1,0:T(8,128)(2,1)}, u32[]{:S(2)}) copy-start(bf16[512,256]{1,0:T(8,128)(2,1)} %param.21) | copy-start | bytes 786436
  6.5 65.1 %all-gather.7.cloned.1.call-start = ((), (), s32[]{:S(2)}) async-start(), calls=%async_computation.2 | async-start | bytes 3538944 | tf_op jit(solution)/shard_map/all_gather | solution.py:101
  9.7 100.5 %all-gather.9.cloned.1.call-start = ((), (), s32[]{:S(2)}) async-start(), calls=%async_computation.3 | async-start | bytes 5242880 | tf_op jit(solution)/shard_map/all_gather | solution.py:116
  10.5 160.9 %all-gather.13.cloned.1.call-start = ((), (), s32[]{:S(2)}) async-start(), calls=%async_computation.5 | async-start | bytes 3538944 | tf_op jit(solution)/shard_map/all_gather | solution.py:124
  11.2 181.0 %all-gather.11.cloned.1.call-start = ((), (), s32[]{:S(2)}) async-start(), calls=%async_computation.4 | async-start | bytes 1966080 | tf_op jit(solution)/shard_map/all_gather | solution.py:121
  76.1 1.0 copy-start.1
  77.2 2.4 copy-start
  77.2 2.4 copy-start.3
  110.2 3.5 copy-start.5
  114.6 138.5 %all-gather.15.cloned.1.call-start = ((), (), s32[]{:S(2)}) async-start(), calls=%async_computation.6 | async-start | bytes 3538944 | tf_op jit(solution)/shard_map/all_gather | solution.py:128
  115.2 201.0 %all-gather.17.cloned.1.call-start = ((), (), s32[]{:S(2)}) async-start(), calls=%async_computation.7 | async-start | bytes 3538944 | tf_op jit(solution)/shard_map/all_gather | solution.py:132
  115.8 235.0 %reduce-scatter.2.cloned.1.call-start = ((), (), s32[]{:S(2)}) async-start(), calls=%async_computation.8 | async-start | bytes 1966080 | tf_op jit(solution)/shard_map/reduce_scatter | solution.py:134
  192.2 124.0 %copy-start.8 = (bf16[384,2048]{1,0:T(8,128)(2,1)S(1)}, bf16[384,2048]{1,0:T(8,128)(2,1)}, u32[]{:S(2)}) copy-start(bf16[384,2048]{1,0:T(8,128)(2,1)} %all-gather.11.cloned.1.call-done) | copy-start | bytes 4718596
  323.7 30.0 %copy-start.7 = (f32[2048]{0:T(1024)S(1)}, f32[2048]{0:T(1024)}, u32[]{:S(2)}) copy-start(f32[2048]{0:T(1024)} %param.29) | copy-start | bytes 24580
Sparse Core Ops, SparseCore 0:
  9.8 61.7 all-gather.6
  73.2 36.9 all-gather.8
  112.4 58.9 all-gather.12
  172.8 19.3 all-gather.10
  194.2 58.9 all-gather.14
  255.1 61.0 all-gather.16
  323.8 26.9 reduce-scatter.1
where the time goes:
time: 366 us; the launch traced here: 363 us
  waiting for transfers between devices  275 us (75%)
  blocking collectives  35.3 us (10%)
  matrix products  25.3 us (7%)
  between operations  13.6 us (4%)
  other arithmetic  13 us (4%)
    all_gather x1, waiting for transfers between devices, per_device(): lax.all_gather(w_down, 'sp', axis=1, tiled=True)  63 us
    all_gather x1, waiting for transfers between devices, per_device(): lax.all_gather(w_up, 'sp', axis=0, tiled=True)  56.1 us
    all_gather x1, waiting for transfers between devices, per_device(): lax.all_gather(w_gate, 'sp', axis=0, tiled=True)  55.5 us
    all_gather x1, waiting for transfers between devices, per_device(): lax.all_gather(normed, 'sp', axis=0, tiled=True)  34 us
    reduce_scatter x1, waiting for transfers between devices, per_device(): lax.psum_scatter(terms.astype(jnp.bfloat16), 'tp', scatter_dimension=0, t...  27.1 us
    all_gather x1, blocking collectives, per_device(): lax.all_gather(key_turned, 'sp', axis=0, tiled=True)  25.2 us
    all_gather x1, waiting for transfers between devices, per_device(): all_rows = lax.all_gather(mixed, 'tp', axis=0, tiled=True)  20.8 us
    all_gather x1, waiting for transfers between devices, per_device(): whole_proj = lax.all_gather(out_proj, 'tp', axis=0, tiled=True)  15.7 us
  transfers between devices with their start and end apart: 7, of which 7 were waited for; matrix products, arithmetic and copies ran while one was open for 6% of the time, Pallas kernels for 0%

commit v1 on v0

v1 whole, which is shorter than its diff:
```python
import functools

import jax
import jax.numpy as jnp
from jax import lax
from jax.experimental import pallas as pl
from jax.experimental.pallas import tpu as pltpu
from jax.sharding import PartitionSpec as P

theta_base = 10000.0
residual_weight = 8.0**0.25
norm_floor = 1.0
big_negative = -1e30


def rotate(vector, first_row):
    half = vector.shape[-1] // 2
    rates = theta_base ** (-2.0 * jnp.arange(half, dtype=jnp.float32) / vector.shape[-1])
    places = (first_row + jnp.arange(vector.shape[0], dtype=jnp.int32)).astype(jnp.float32)
    angle = places[:, None] * rates[None, :]
    angle = angle.reshape((vector.shape[0],) + (1,) * (vector.ndim - 2) + (half,))
    cosine = jnp.cos(angle)
    sine = jnp.sin(angle)
    left = vector[..., :half]
    right = vector[..., half:]
    return jnp.concatenate([left * cosine - right * sine, left * sine + right * cosine], axis=-1)


def latent_norm(latent, latent_gain):
    wide = latent.astype(jnp.float32)
    factor = lax.rsqrt(jnp.mean(wide * wide, axis=-1, keepdims=True) + norm_floor)
    return (wide * factor * latent_gain).astype(jnp.bfloat16)


def layer_norm(values, gain):
    centre = jnp.mean(values, axis=-1, keepdims=True)
    centred = values - centre
    spread = jnp.mean(centred * centred, axis=-1, keepdims=True)
    return centred * lax.rsqrt(spread + norm_floor) * gain


mesh_id = pl.DeviceIdType.MESH
bf16 = jnp.bfloat16
f32 = jnp.float32


def layer_kernel(
    chain,
    teams,
    scale,
    qcat,
    latent_in,
    key_up,
    value_up,
    proj_in,
    stream,
    mix_gain,
    gate_in,
    up_in,
    down_in,
    mlp_gain,
    result,
    lat,
    gate,
    up,
    down,
    proj,
    heads_out,
    heads_in,
    rows,
    hidden,
    terms,
    arrived,
    wide,
    top,
    total,
    weighted,
    local_sem,
    lat_recv,
    lat_up,
    lat_side,
    lat_core,
    w_recv,
    w_side,
    w_up,
    w_down,
    proj_recv,
    proj_send,
    head_recv,
    head_send,
    row_recv,
    row_send,
    term_recv,
    term_send,
):
    sp = lax.axis_index("sp")
    t = lax.axis_index("tp")
    q = sp // 2
    p = sp % 2
    other = 1 - p
    half = t % 2
    mate = t + 1 - 2 * half
    group = 2 * teams
    mine = p * teams + t
    last = chain - 1
    head_count = qcat.shape[0]
    head_dim = value_up.shape[1] // head_count
    block_rows = qcat.shape[1]
    width = value_up.shape[0]
    has_up = q < last
    has_down = q > 0

    def place(pp, tt, qq=None):
        return ((q if qq is None else qq) * 2 + pp, tt)

    def remote(source, target, send, recv, device):
        return pltpu.make_async_remote_copy(
            src_ref=source,
            dst_ref=target,
            send_sem=send,
            recv_sem=recv,
            device_id=device,
            device_id_type=mesh_id,
        )

    barrier = pltpu.get_barrier_semaphore()
    for step in range(1, group):
        index = lax.rem(mine + step, group)
        pl.semaphore_signal(
            barrier, inc=1, device_id=place(index // teams, index % teams), device_id_type=mesh_id
        )

    @pl.when(has_up)
    def _():
        pl.semaphore_signal(barrier, inc=1, device_id=place(p, t, q + 1), device_id_type=mesh_id)

    @pl.when(has_down)
    def _():
        pl.semaphore_signal(barrier, inc=1, device_id=place(p, t, q - 1), device_id_type=mesh_id)

    peers = group - 1 + jnp.where(has_up, 1, 0) + jnp.where(has_down, 1, 0)
    pl.semaphore_wait(barrier, peers)

    def lat_to_up(j, source):
        return remote(
            source, lat.at[j, p, half], lat_up.at[j], lat_recv.at[j, p, half], place(p, t, q + 1)
        )

    def lat_to_side(j, source):
        return remote(
            source, lat.at[j, p, half], lat_side.at[j], lat_recv.at[j, p, half], place(other, t)
        )

    def lat_to_core(j, pp):
        spot = lat.at[j, pp, half]
        return remote(spot, spot, lat_core.at[j, pp], lat_recv.at[j, pp, half], place(p, mate))

    def lat_wait(j, pp, hh):
        spot = lat.at[j, pp, hh]
        remote(spot, spot, lat_up.at[0], lat_recv.at[j, pp, hh], place(p, mate)).wait_recv()

    stores = (gate, up, down)
    hidden_half = gate.shape[3]

    def piece(w, which):
        start = pl.multiple_of(which * hidden_half, 128)
        if w == 0:
            return gate_in.at[:, pl.ds(start, hidden_half)]
        if w == 1:
            return up_in.at[:, pl.ds(start, hidden_half)]
        return down_in.at[pl.ds(start, hidden_half), :]

    def w_to_side(w):
        return remote(
            piece(w, other),
            stores[w].at[q, p],
            w_side.at[w],
            w_recv.at[w, q, p],
            place(other, t),
        )

    def w_to_up(w, j, pp):
        spot = stores[w].at[j, pp]
        return remote(spot, spot, w_up.at[w, j, pp], w_recv.at[w, j, pp], place(p, t, q + 1))

    def w_to_down(w, j, pp):
        spot = stores[w].at[j, pp]
        return remote(spot, spot, w_down.at[w, j, pp], w_recv.at[w, j, pp], place(p, t, q - 1))

    def w_wait(w, j, pp):
        spot = stores[w].at[j, pp]
        remote(spot, spot, w_up.at[w, 0, 0], w_recv.at[w, j, pp], place(p, mate)).wait_recv()

    def w_own(w):
        return pltpu.make_async_copy(piece(w, p), stores[w].at[q, p], local_sem.at[1 + w])

    own_lat = pltpu.make_async_copy(latent_in, lat.at[q, p], local_sem.at[0])
    own_proj = pltpu.make_async_copy(proj_in, proj.at[t], local_sem.at[4])

    def proj_to(step):
        tt = lax.rem(t + step, teams)
        return remote(
            proj_in, proj.at[t], proj_send.at[step], proj_recv.at[step], place(p, tt)
        )

    own_lat.start()
    w_own(0).start()
    w_own(1).start()
    w_own(2).start()

    @pl.when(has_up)
    def _():
        lat_to_up(q, latent_in.at[half]).start()

    lat_to_side(q, latent_in.at[half]).start()
    for w in range(3):
        w_to_side(w).start()
    own_proj.start()
    for step in range(1, teams):
        proj_to(step).start()
    for w in range(3):
        w_own(w).wait()

        @pl.when(has_down)
        def _():
            w_to_down(w, q, p).start()

    top[...] = jnp.full_like(top, big_negative)
    total[...] = jnp.zeros_like(total)
    weighted[...] = jnp.zeros_like(weighted)

    def attend(j, pp, diagonal):
        block = lat[j, pp].reshape(block_rows, lat.shape[4])
        normed = block[:, :width]
        rotary = block[:, width:]
        keys = jnp.dot(normed, key_up[...], preferred_element_type=f32).astype(bf16)
        values = jnp.dot(normed, value_up[...], preferred_element_type=f32).astype(bf16)
        for h in range(head_count):
            span = slice(h * head_dim, (h + 1) * head_dim)
            both = jnp.concatenate([keys[:, span], rotary], axis=1)
            score = (
                lax.dot_general(
                    qcat[h], both, (((1,), (1,)), ((), ())), preferred_element_type=f32
                )
                * scale
            )
            if diagonal:
                across = lax.broadcasted_iota(jnp.int32, score.shape, 1)
                along = lax.broadcasted_iota(jnp.int32, score.shape, 0)
                score = jnp.where(across <= along, score, big_negative)
            old = top[h]
            new = jnp.maximum(old, jnp.max(score, axis=1, keepdims=True))
            powers = jnp.exp(score - new)
            shrink = jnp.exp(old - new)
            total[h] = total[h] * shrink + jnp.sum(powers, axis=1, keepdims=True)
            weighted[h] = weighted[h] * shrink + jnp.dot(
                powers.astype(bf16), values[:, span], preferred_element_type=f32
            )
            top[h] = new

    own_lat.wait()
    attend(q, p, True)

    for w in range(3):
        w_wait(w, q, other)

        @pl.when(has_down)
        def _():
            w_to_down(w, q, other).start()

    lat_wait(q, other, half)
    lat_to_core(q, other).start()

    def lat_step(s, carry):
        j = q - s

        @pl.when(j >= 0)
        def _():
            lat_wait(j, p, half)

            @pl.when(has_up)
            def _():
                lat_to_up(j, lat.at[j, p, half]).start()

            lat_to_side(j, lat.at[j, p, half]).start()
            lat_to_core(j, p).start()
            lat_wait(j, other, half)
            lat_to_core(j, other).start()

        return carry

    lax.fori_loop(1, chain, lat_step, 0)

    @pl.when(has_up)
    def _():
        for w in range(3):
            w_to_up(w, q, p).start()
            w_to_up(w, q, other).start()

    lat_wait(q, other, 1 - half)

    def whole_block(index, carry):
        j = q - (index + 1) // 2
        pp = jnp.where(index % 2 == 1, p, other)

        @pl.when(j >= 0)
        def _():
            @pl.when(index > 0)
            def _():
                lat_wait(j, pp, 1 - half)

            @pl.when((index > 0) | (p == 1))
            def _():
                attend(j, pp, False)

        return carry

    lax.fori_loop(0, 2 * chain - 1, whole_block, 0)

    part = block_rows // teams
    for h in range(head_count):
        span = slice(h * head_dim, (h + 1) * head_dim)
        done = (weighted[h] / total[h]).astype(bf16)
        heads_out[:, :, span] = done.reshape(teams, part, head_dim)

    def head_to(step):
        tt = lax.rem(t + step, teams)
        return remote(
            heads_out.at[tt], heads_in.at[t], head_send.at[step], head_recv.at[step], place(p, tt)
        )

    for step in range(1, teams):
        head_to(step).start()
    heads_in[t] = heads_out[t]

    def w_step(kinds, s):
        for w in kinds:
            for k in range(2):

                @pl.when(q - s >= 0)
                def _():
                    w_wait(w, q - s, k)

                    @pl.when(has_up)
                    def _():
                        w_to_up(w, q - s, k).start()

                @pl.when(q + s <= last)
                def _():
                    w_wait(w, q + s, k)

                    @pl.when(has_down)
                    def _():
                        w_to_down(w, q + s, k).start()

    def w_steps(kinds, first, end):
        def body(s, carry):
            w_step(kinds, s)
            return carry

        lax.fori_loop(first, end, body, 0)

    w_steps((0, 1), 1, 2)

    own_proj.wait()
    for step in range(1, teams):
        head_to(step).wait_recv()
        proj_to(step).wait_recv()

    def project(k, carry):
        wide[...] += jnp.dot(heads_in[k], proj[k], preferred_element_type=f32)
        return carry

    wide[...] = residual_weight * stream[...].astype(f32)
    lax.fori_loop(0, teams, project, 0)
    rows[mine] = layer_norm(wide[...], mix_gain[...]).astype(bf16)

    held = [(p, t)]
    slot = 0
    bits = []
    bit = 2
    while bit < teams:
        bits.append(bit)
        bit *= 2
    for stage in bits + [0, 1]:

        def flip(pp, tt):
            if stage == 0:
                return 1 - pp, tt
            return pp, jnp.where((tt // stage) % 2 == 0, tt + stage, tt - stage)

        partner = place(*flip(p, t))
        batch = []
        for pp, tt in held:
            spot = rows.at[pp * teams + tt]
            batch.append(
                remote(spot, spot, row_send.at[slot], row_recv.at[slot], partner)
            )
            slot += 1
        for copy in batch:
            copy.start()
        if stage == 0:
            w_steps((0, 1), 2, chain)
        for copy in batch:
            copy.wait()
        held = held + [flip(pp, tt) for pp, tt in held]

    def feed(k, carry):
        here = rows[pl.ds(2 * k, 2)].reshape(2 * part, rows.shape[2])
        gate_sum = jnp.dot(
            here, gate[...].reshape(-1, hidden_half), preferred_element_type=f32
        )
        up_sum = jnp.dot(here, up[...].reshape(-1, hidden_half), preferred_element_type=f32)
        value = gate_sum / (1.0 + jnp.exp(-gate_sum)) * up_sum
        hidden[pl.ds(2 * k, 2)] = value.astype(bf16).reshape(2, part, hidden_half)
        return carry

    lax.fori_loop(0, group // 2, feed, 0)

    def term_to(j, step):
        index = lax.rem(mine + step, group)
        return remote(
            terms.at[j, index],
            arrived.at[j, mine],
            term_send.at[j, step],
            term_recv.at[j, step],
            place(index // teams, index % teams),
        )

    def lower(j):
        weights = jnp.concatenate([down[j, 0], down[j, 1]], axis=1)
        product = jnp.dot(
            hidden[...].reshape(group * part, hidden_half), weights, preferred_element_type=f32
        )
        terms[j] = product.astype(bf16).reshape(group, part, product.shape[1])
        for step in range(1, group):
            term_to(j, step).start()

    lower(q)

    def lower_step(s, carry):
        w_step((2,), s)

        def one(side, inner):
            j = jnp.where(side == 0, q - s, q + s)

            @pl.when((j >= 0) & (j <= last))
            def _():
                lower(j)

            return inner

        lax.fori_loop(0, 2, one, 0)
        return carry

    lax.fori_loop(1, chain, lower_step, 0)

    def collect(j, carry):
        for step in range(1, group):
            term_to(j, step).wait()
        return carry

    lax.fori_loop(0, chain, collect, 0)
    span_width = terms.shape[3]
    for j in range(chain):
        arrived[j, mine] = terms[j, mine]
        lowered = arrived[j, 0].astype(f32)
        for k in range(1, group):
            lowered = lowered + arrived[j, k].astype(f32)
        span = slice(j * span_width, (j + 1) * span_width)
        wide[:, span] = residual_weight * rows[mine, :, span].astype(f32) + 0.5 * lowered
    result[...] = layer_norm(wide[...], mlp_gain[...]).astype(bf16)

    for w in range(3):
        w_to_side(w).wait_send()
    for step in range(1, teams):
        proj_to(step).wait_send()
        head_to(step).wait_send()

    def drain(j, carry):
        @pl.when(has_up & (j <= q))
        def _():
            lat_to_up(j, lat.at[j, p, half]).wait_send()
            for w in range(3):
                for k in range(2):
                    w_to_up(w, j, k).wait_send()

        @pl.when(has_down & (j >= q))
        def _():
            for w in range(3):
                for k in range(2):
                    w_to_down(w, j, k).wait_send()

        @pl.when(j <= q)
        def _():
            lat_to_side(j, lat.at[j, p, half]).wait_send()
            lat_to_core(j, other).wait_send()

        @pl.when(j < q)
        def _():
            lat_to_core(j, p).wait_send()

        return carry

    lax.fori_loop(0, chain, drain, 0)


def per_device(
    chain,
    teams,
    queries_nope,
    queries_rope,
    latent,
    rope_key,
    latent_gain,
    key_up,
    value_up,
    out_proj,
    stream,
    mix_gain,
    w_gate,
    w_up,
    w_down,
    mlp_gain,
):
    row_count, head_count, head_dim = queries_nope.shape
    rope_dim = queries_rope.shape[2]
    first_row = lax.axis_index("sp") * row_count
    query_turned = rotate(queries_rope.astype(jnp.float32), first_row).astype(jnp.bfloat16)
    key_turned = rotate(rope_key.astype(jnp.float32), first_row).astype(jnp.bfloat16)
    normed = latent_norm(latent, latent_gain)
    scale = (head_dim + rope_dim) ** (-0.5)
    spare = -rope_dim % 128
    qcat = jnp.concatenate(
        [queries_nope, query_turned, jnp.zeros((row_count, head_count, spare), bf16)], axis=2
    ).transpose(1, 0, 2)
    latent_in = jnp.concatenate(
        [normed, key_turned, jnp.zeros((row_count, spare), bf16)], axis=1
    ).reshape(2, row_count // 2, -1)
    width = latent_in.shape[2]
    model, hidden_here = w_gate.shape[0] * 2 * chain, w_gate.shape[1]
    group = 2 * teams
    part = row_count // teams
    half_hidden = hidden_here // 2
    deep = w_gate.shape[0]
    slim = w_down.shape[1]
    stages = group - 1
    dma = pltpu.SemaphoreType.DMA
    vmem = pl.BlockSpec(memory_space=pltpu.VMEM)
    hbm = pl.BlockSpec(memory_space=pltpu.HBM)
    return pl.pallas_call(
        functools.partial(layer_kernel, chain, teams, scale),
        out_shape=jax.ShapeDtypeStruct((part, model), bf16),
        in_specs=[vmem, hbm, vmem, vmem, hbm, vmem, vmem, hbm, hbm, hbm, vmem],
        out_specs=vmem,
        scratch_shapes=[
            pltpu.VMEM((chain, 2, 2, row_count // 2, width), bf16),
            pltpu.VMEM((chain, 2, deep, half_hidden), bf16),
            pltpu.VMEM((chain, 2, deep, half_hidden), bf16),
            pltpu.VMEM((chain, 2, half_hidden, slim), bf16),
            pltpu.VMEM((teams,) + out_proj.shape, bf16),
            pltpu.VMEM((teams, part, head_count * head_dim), bf16),
            pltpu.VMEM((teams, part, head_count * head_dim), bf16),
            pltpu.VMEM((group, part, model), bf16),
            pltpu.VMEM((group, part, half_hidden), bf16),
            pltpu.VMEM((chain, group, part, 2 * slim), bf16),
            pltpu.VMEM((chain, group, part, 2 * slim), bf16),
            pltpu.VMEM((part, model), f32),
            pltpu.VMEM((head_count, row_count, 1), f32),
            pltpu.VMEM((head_count, row_count, 1), f32),
            pltpu.VMEM((head_count, row_count, head_dim), f32),
            dma((5,)),
            dma((chain, 2, 2)),
            dma((chain,)),
            dma((chain,)),
            dma((chain, 2)),
            dma((3, chain, 2)),
            dma((3,)),
            dma((3, chain, 2)),
            dma((3, chain, 2)),
            dma((teams,)),
            dma((teams,)),
            dma((teams,)),
            dma((teams,)),
            dma((stages,)),
            dma((stages,)),
            dma((chain, group)),
            dma((chain, group)),
        ],
        compiler_params=pltpu.CompilerParams(
            collective_id=0, has_side_effects=True, vmem_limit_bytes=60 * 1024 * 1024
        ),
    )(
        qcat,
        latent_in,
        key_up,
        value_up,
        out_proj,
        stream,
        mix_gain.reshape(1, -1),
        w_gate,
        w_up,
        w_down,
        mlp_gain.reshape(1, -1),
    )


def solution(mesh):
    return jax.shard_map(
        functools.partial(per_device, mesh.shape["sp"] // 2, mesh.shape["tp"]),
        mesh=mesh,
        in_specs=(
            P("sp", "tp", None),
            P("sp", "tp", None),
            P("sp", None),
            P("sp", None),
            P(),
            P(None, "tp"),
            P(None, "tp"),
            P("tp", None),
            P(("sp", "tp"), None),
            P(),
            P("sp", "tp"),
            P("sp", "tp"),
            P("tp", "sp"),
            P(),
        ),
        out_specs=P(("sp", "tp"), None),
        check_vma=False,
    )
```

time: 366 us -> 153 us (0.42)
  waiting for transfers between devices: 275 us -> 0 us
  Pallas kernels: 0 us -> 145 us
  blocking collectives: 35.3 us -> 0 us
  matrix products: 25.3 us -> 0 us
  between operations: 13.6 us -> 0.11 us
  other arithmetic: 13 us -> 3.45 us
  local copies, waits for them, and re-layouts: 0.35 us -> 4.67 us
    all_gather x6 -> x0, waiting for transfers between devices: 245 us -> none  [the longest x1 63 us: per_device(): lax.all_gather(w_down, 'sp', axis=1, tiled=True)]
    pallas_call x0 -> x1, Pallas kernels: none -> 145 us  [per_device(): pl.pallas_call(functools.partial(layer_kernel, chain, teams, scale), out_...]
    reduce_scatter x1 -> x0, waiting for transfers between devices: 27.1 us -> none  [per_device(): lax.psum_scatter(terms.astype(jnp.bfloat16), 'tp', scatter_dimension=0, t...]
    dot_general x8 -> x0, matrix products: 25.3 us -> none  [the longest x1 7.45 us: per_device(): jnp.dot(hidden, lax.all_gather(w_down, 'sp', axis=1, tiled=True), preferr...]
    all_gather x1 -> x0, blocking collectives: 25.2 us -> none  [per_device(): lax.all_gather(key_turned, 'sp', axis=0, tiled=True)]
    all_to_all x1 -> x0, blocking collectives: 10.1 us -> none  [per_device(): lax.all_to_all(attended, 'tp', split_axis=0, concat_axis=1, tiled=True)]
    reduce_sum x4 -> x0, other arithmetic: 4.59 us -> none  [the longest x2 1.69 us: layer_norm(): spread = jnp.mean(centred * centred, axis=-1, keepdims=True)]
    convert_element_type x4 -> x0, other arithmetic: 4.12 us -> none  [the longest x1 2.19 us: per_device(): layer_norm(residual_weight * mixed.astype(jnp.float32) + 0.5 * lowered, m...]
  transfers between devices with their start and end apart: 7 -> 0, of which waited for: 7 -> 0; matrix products, arithmetic and copies ran while one was open for 6% -> 0% of each run, Pallas kernels for 0% -> 0%
where the time goes in v1:
time: 153 us
  Pallas kernels  145 us (95%)
  local copies, waits for them, and re-layouts  4.67 us (3%)
  other arithmetic  3.45 us (2%)
    pallas_call x1, Pallas kernels, per_device(): pl.pallas_call(functools.partial(layer_kernel, chain, teams, scale), out_...  145 us
    unnamed x11, local copies, waits for them, and re-layouts  4.02 us

profile of v1, /device:TPU:27, one launch (start us, length us, event | category | flops | bytes accessed | tf_op | source)
XLA Modules:
  0.0 153.0 jit_solution(18147538044096315269)
XLA Ops:
  0.0 0.8 convert_element_type.26
  0.8 0.3 subtract_convert_fusion.1
  1.1 0.1 copy.16
  1.2 0.0 copy-start.2
  1.2 0.1 copy.17
  1.4 0.8 copy-done.2
  2.1 0.2 copy.15
  2.3 0.0 copy-start.1
  2.4 0.2 subtract_convert_fusion
  2.6 0.1 pad.7.clone
  2.6 0.6 copy-done.1
  3.3 0.0 copy-start
  3.3 0.9 maximum_bitcast_fusion.qcat
  4.2 0.1 copy.19
  4.3 0.1 copy.20
  4.5 0.1 pad.3.clone
  4.5 0.0 copy-done
  4.5 0.2 fusion
  4.7 0.0 copy-start.3
  4.7 0.7 copy-done.3
  5.4 0.2 fusion.2
  5.6 0.9 maximum_maximum_fusion
  6.5 144.8 %shard_map.136 = bf16[96,2048]{1,0:T(8,128)(2,1)} custom-call(bf16[2,384,256]{2,1,0:T(8,128)(2,1)} %maximum_bitcast_fusion.qcat, bf16[2,192,640]{2,1,0:T(8,128)(2,1)} %bitcast.5, bf16[512,256]{1,0:T(8,128)(2,1)} %key_up.1, bf16[512,256]{1,0:T(8,128)(2,1)} %value_up.1, bf16[256,2048]{1,0:T(8,128)(2,1)} %proj_in.1, bf16[96,2048]{1,0:T(8,128)(2,1)} %stream.1, ...), custom_call_target="tpu_custom_call" | custom-call | tf_op jit(solution)/shard_map/pallas_call | solution.py:551
  151.3 1.8 %copy.22 = bf16[96,2048]{1,0:T(8,128)(2,1)} copy(bf16[96,2048]{1,0:T(8,128)(2,1)} %shard_map.136) | data formatting | bytes 786432
  (6 shorter events, 0.1 us)
Async XLA Ops:
  1.2 0.9 copy-start.2
  2.3 0.9 copy-start.1
  3.3 1.2 copy-start
  4.7 0.7 copy-start.3

commit v2 on v1

--- a/solution.py
+++ b/solution.py
@@ -69,6 +69,8 @@
     heads_in,
     rows,
     hidden,
+    terms_out,
+    mate_in,
     terms,
     arrived,
     wide,
@@ -90,6 +92,8 @@
     head_send,
     row_recv,
     row_send,
+    mate_recv,
+    mate_send,
     term_recv,
     term_send,
 ):
@@ -101,7 +105,8 @@
     half = t % 2
     mate = t + 1 - 2 * half
     group = 2 * teams
-    mine = p * teams + t
+    mine = half * teams + p * (teams // 2) + t // 2
+    own_class = half * teams
     last = chain - 1
     head_count = qcat.shape[0]
     head_dim = value_up.shape[1] // head_count
@@ -124,8 +129,9 @@
         )
 
     barrier = pltpu.get_barrier_semaphore()
+    place_here = p * teams + t
     for step in range(1, group):
-        index = lax.rem(mine + step, group)
+        index = lax.rem(place_here + step, group)
         pl.semaphore_signal(
             barrier, inc=1, device_id=place(index // teams, index % teams), device_id_type=mesh_id
         )
@@ -199,9 +205,14 @@
 
     def proj_to(step):
         tt = lax.rem(t + step, teams)
-        return remote(
-            proj_in, proj.at[t], proj_send.at[step], proj_recv.at[step], place(p, tt)
-        )
+        return remote(proj_in, proj.at[t], proj_send.at[step], proj_recv.at[step], place(p, tt))
+
+    def proj_mate():
+        return remote(proj_in, proj.at[t], proj_send.at[1], proj_recv.at[1], place(p, mate))
+
+    def proj_pass(step):
+        spot = proj.at[lax.rem(t - step + teams, teams)]
+        return remote(spot, spot, proj_send.at[step + 1], proj_recv.at[step + 1], place(p, mate))
 
     own_lat.start()
     w_own(0).start()
@@ -216,8 +227,9 @@
     for w in range(3):
         w_to_side(w).start()
     own_proj.start()
-    for step in range(1, teams):
+    for step in range(2, teams, 2):
         proj_to(step).start()
+    proj_mate().start()
     for w in range(3):
         w_own(w).wait()
 
@@ -293,7 +305,7 @@
 
     @pl.when(has_up)
     def _():
-        for w in range(3):
+        for w in range(2):
             w_to_up(w, q, p).start()
             w_to_up(w, q, other).start()
 
@@ -360,12 +372,22 @@
 
         lax.fori_loop(first, end, body, 0)
 
+    for step in range(2, teams, 2):
+        proj_to(step).wait_recv()
+        proj_pass(step).start()
     w_steps((0, 1), 1, 2)
 
+    @pl.when(has_up)
+    def _():
+        w_to_up(2, q, p).start()
+        w_to_up(2, q, other).start()
+
     own_proj.wait()
+    proj_mate().wait_recv()
     for step in range(1, teams):
         head_to(step).wait_recv()
-        proj_to(step).wait_recv()
+    for step in range(2, teams, 2):
+        proj_pass(step).wait_recv()
 
     def project(k, carry):
         wide[...] += jnp.dot(heads_in[k], proj[k], preferred_element_type=f32)
@@ -375,35 +397,37 @@
     lax.fori_loop(0, teams, project, 0)
     rows[mine] = layer_norm(wide[...], mix_gain[...]).astype(bf16)
 
-    held = [(p, t)]
-    slot = 0
-    bits = []
+    stages = []
     bit = 2
     while bit < teams:
-        bits.append(bit)
+        stages.append(bit)
         bit *= 2
-    for stage in bits + [0, 1]:
-
-        def flip(pp, tt):
-            if stage == 0:
-                return 1 - pp, tt
-            return pp, jnp.where((tt // stage) % 2 == 0, tt + stage, tt - stage)
-
-        partner = place(*flip(p, t))
-        batch = []
-        for pp, tt in held:
-            spot = rows.at[pp * teams + tt]
-            batch.append(
-                remote(spot, spot, row_send.at[slot], row_recv.at[slot], partner)
-            )
-            slot += 1
-        for copy in batch:
-            copy.start()
+    stages += [0, 1]
+
+    def flip(stage, pp, tt):
         if stage == 0:
-            w_steps((0, 1), 2, chain)
-        for copy in batch:
-            copy.wait()
-        held = held + [flip(pp, tt) for pp, tt in held]
+            return 1 - pp, tt
+        return pp, jnp.where((tt // stage) % 2 == 0, tt + stage, tt - stage)
+
+    held = [(p, t)]
+    for stage in stages:
+        held = held + [flip(stage, pp, tt) for pp, tt in held]
+
+    def row_copy(i, u):
+        pp, tt = held[u]
+        spot = rows.at[(tt % 2) * teams + pp * (teams // 2) + tt // 2]
+        slot = 2**i - 1 + u
+        partner = place(*flip(stages[i], p, t))
+        return remote(spot, spot, row_send.at[slot], row_recv.at[slot], partner)
+
+    for i in range(len(stages)):
+        row_copy(i, 0).start()
+    for i in range(len(stages)):
+        for u in range(2**i):
+            row_copy(i, u).wait_recv()
+            for later in range(i + 1, len(stages)):
+                row_copy(later, 2**i + u).start()
+    w_steps((0, 1), 2, chain)
 
     def feed(k, carry):
         here = rows[pl.ds(2 * k, 2)].reshape(2 * part, rows.shape[2])
@@ -417,23 +441,40 @@
 
     lax.fori_loop(0, group // 2, feed, 0)
 
+    my_turn = p * (teams // 2) + t // 2
+
+    def term_mate(j):
+        return remote(
+            terms_out.at[j], mate_in.at[j], mate_send.at[j], mate_recv.at[j], place(p, mate)
+        )
+
     def term_to(j, step):
-        index = lax.rem(mine + step, group)
+        index = lax.rem(my_turn + step, teams)
+        pp = index // (teams // 2)
+        tt = 2 * (index % (teams // 2)) + half
         return remote(
             terms.at[j, index],
-            arrived.at[j, mine],
+            arrived.at[j, my_turn],
             term_send.at[j, step],
             term_recv.at[j, step],
-            place(index // teams, index % teams),
+            place(pp, tt),
         )
 
     def lower(j):
         weights = jnp.concatenate([down[j, 0], down[j, 1]], axis=1)
-        product = jnp.dot(
-            hidden[...].reshape(group * part, hidden_half), weights, preferred_element_type=f32
-        )
-        terms[j] = product.astype(bf16).reshape(group, part, product.shape[1])
-        for step in range(1, group):
+
+        def product(first):
+            here = hidden[pl.ds(first, teams)].reshape(teams * part, hidden_half)
+            return jnp.dot(here, weights, preferred_element_type=f32)
+
+        there = product(teams - own_class)
+        terms_out[j] = there.astype(bf16).reshape(teams, part, there.shape[1])
+        term_mate(j).start()
+        kept = product(own_class)
+        term_mate(j).wait_recv()
+        kept = kept.reshape(teams, part, kept.shape[1]) + mate_in[j].astype(f32)
+        terms[j] = kept.astype(bf16)
+        for step in range(1, teams):
             term_to(j, step).start()
 
     lower(q)
@@ -456,16 +497,16 @@
     lax.fori_loop(1, chain, lower_step, 0)
 
     def collect(j, carry):
-        for step in range(1, group):
+        for step in range(1, teams):
             term_to(j, step).wait()
         return carry
 
     lax.fori_loop(0, chain, collect, 0)
     span_width = terms.shape[3]
     for j in range(chain):
-        arrived[j, mine] = terms[j, mine]
+        arrived[j, my_turn] = terms[j, my_turn]
         lowered = arrived[j, 0].astype(f32)
-        for k in range(1, group):
+        for k in range(1, teams):
             lowered = lowered + arrived[j, k].astype(f32)
         span = slice(j * span_width, (j + 1) * span_width)
         wide[:, span] = residual_weight * rows[mine, :, span].astype(f32) + 0.5 * lowered
@@ -473,11 +514,19 @@
 
     for w in range(3):
         w_to_side(w).wait_send()
+    proj_mate().wait_send()
+    for step in range(2, teams, 2):
+        proj_to(step).wait_send()
+        proj_pass(step).wait_send()
     for step in range(1, teams):
-        proj_to(step).wait_send()
         head_to(step).wait_send()
+    for i in range(len(stages)):
+        for u in range(2**i):
+            row_copy(i, u).wait_send()
 
     def drain(j, carry):
+        term_mate(j).wait_send()
+
         @pl.when(has_up & (j <= q))
         def _():
             lat_to_up(j, lat.at[j, p, half]).wait_send()
@@ -563,8 +612,10 @@
             pltpu.VMEM((teams, part, head_count * head_dim), bf16),
             pltpu.VMEM((group, part, model), bf16),
             pltpu.VMEM((group, part, half_hidden), bf16),
-            pltpu.VMEM((chain, group, part, 2 * slim), bf16),
-            pltpu.VMEM((chain, group, part, 2 * slim), bf16),
+            pltpu.VMEM((chain, teams, part, 2 * slim), bf16),
+            pltpu.VMEM((chain, teams, part, 2 * slim), bf16),
+            pltpu.VMEM((chain, teams, part, 2 * slim), bf16),
+            pltpu.VMEM((chain, teams, part, 2 * slim), bf16),
             pltpu.VMEM((part, model), f32),
             pltpu.VMEM((head_count, row_count, 1), f32),
             pltpu.VMEM((head_count, row_count, 1), f32),
@@ -584,8 +635,10 @@
             dma((teams,)),
             dma((stages,)),
             dma((stages,)),
-            dma((chain, group)),
-            dma((chain, group)),
+            dma((chain,)),
+            dma((chain,)),
+            dma((chain, teams)),
+            dma((chain, teams)),
         ],
         compiler_params=pltpu.CompilerParams(
             collective_id=0, has_side_effects=True, vmem_limit_bytes=60 * 1024 * 1024

time: 153 us -> 134 us (0.88)
  Pallas kernels: 145 us -> 125 us
    pallas_call x1, Pallas kernels: 145 us -> 125 us  [per_device(): pl.pallas_call(functools.partial(layer_kernel, chain, teams, scale), out_...]
where the time goes in v2:
time: 134 us; the launch traced here: 133 us
  Pallas kernels  125 us (93%)
  local copies, waits for them, and re-layouts  4.67 us (3%)
  other arithmetic  3.45 us (3%)
    pallas_call x1, Pallas kernels, per_device(): pl.pallas_call(functools.partial(layer_kernel, chain, teams, scale), out_...  125 us
    unnamed x11, local copies, waits for them, and re-layouts  4.02 us

profile of v2, /device:TPU:27, one launch (start us, length us, event | category | flops | bytes accessed | tf_op | source)
XLA Modules:
  0.0 133.1 jit_solution(17950661350035535588)
XLA Ops:
  0.0 0.8 convert_element_type.26
  0.8 0.3 subtract_convert_fusion.1
  1.1 0.1 copy.16
  1.2 0.0 copy-start.2
  1.2 0.1 copy.17
  1.4 0.8 copy-done.2
  2.1 0.2 copy.15
  2.3 0.0 copy-start.1
  2.4 0.2 subtract_convert_fusion
  2.6 0.1 pad.7.clone
  2.6 0.6 copy-done.1
  3.3 0.0 copy-start
  3.3 0.9 maximum_bitcast_fusion.qcat
  4.2 0.1 copy.19
  4.3 0.1 copy.20
  4.5 0.1 pad.3.clone
  4.5 0.0 copy-done
  4.5 0.2 fusion
  4.7 0.0 copy-start.3
  4.7 0.7 copy-done.3
  5.4 0.2 fusion.2
  5.6 0.9 maximum_maximum_fusion
  6.5 124.8 %shard_map.136 = bf16[96,2048]{1,0:T(8,128)(2,1)} custom-call(bf16[2,384,256]{2,1,0:T(8,128)(2,1)} %maximum_bitcast_fusion.qcat, bf16[2,192,640]{2,1,0:T(8,128)(2,1)} %bitcast.5, bf16[512,256]{1,0:T(8,128)(2,1)} %key_up.1, bf16[512,256]{1,0:T(8,128)(2,1)} %value_up.1, bf16[256,2048]{1,0:T(8,128)(2,1)} %proj_in.1, bf16[96,2048]{1,0:T(8,128)(2,1)} %stream.1, ...), custom_call_target="tpu_custom_call" | custom-call | tf_op jit(solution)/shard_map/pallas_call | solution.py:600
  131.3 1.8 %copy.22 = bf16[96,2048]{1,0:T(8,128)(2,1)} copy(bf16[96,2048]{1,0:T(8,128)(2,1)} %shard_map.136) | data formatting | bytes 786432
  (6 shorter events, 0.1 us)
Async XLA Ops:
  1.2 0.9 copy-start.2
  2.3 0.9 copy-start.1
  3.3 1.2 copy-start
  4.7 0.7 copy-start.3
